TPU v7x, 32 devices: a whole 2x2x4 slice. The times are simulated.
32 devices in a mesh: sp: 8 (over z, y), tp: 4 (over x, core).
Axes of the slice: x: 2, y: 2, z: 4, core: 2. Of those that a mesh axis runs over, the one named last changes fastest.
Arguments:
- tokens: bfloat16 [1024, 2048], P(('sp', 'tp')), may hold values from -6 to 6
- doc_lengths: int32 [16], replicated, may hold values from 1 to 640, 1024 in all
- query_down: bfloat16 [2048, 512], replicated, may hold values from -0.125 to 0.125
- latent_down: bfloat16 [2048, 256], replicated, may hold values from -0.125 to 0.125
- rope_down: bfloat16 [2048, 32], replicated, may hold values from -0.125 to 0.125
- query_latent_gain: float32 [512], replicated, may hold values from 0.1 to 1.9
- latent_gain: float32 [256], replicated, may hold values from 0.1 to 1.9
- query_up: bfloat16 [512, 768], P(None, 'tp'), may hold values from -0.25 to 0.25
- key_up: bfloat16 [256, 512], P(None, 'tp'), may hold values from -0.375 to 0.375
- value_up: bfloat16 [256, 512], P(None, 'tp'), may hold values from -0.375 to 0.375
- query_gain: float32 [96], replicated, may hold values from 0.5 to 15
- key_gain: float32 [96], replicated, may hold values from 0.5 to 15
- output_gain: float32 [512], replicated, may hold values from 0.1 to 1.9
- output_weight: bfloat16 [512, 2048], P(None, 'tp'), may hold values from -0.25 to 0.25
Outputs:
- layer_output: bfloat16 [1024, 2048], P('sp', 'tp')
- log_totals: float32 [8, 1024], P('tp', 'sp')
Inputs may be any that keep to these rules, and one draw needn't show every extreme that they name: `doc_lengths`: the lengths sum to 1024; the longest is exactly 640.
All inputs are finite; a program needn't handle non-finite values.
Results may differ from a plain program's by a relative error of at most 0.019.
The roundings to bfloat16 on the way count: a program that leaves them out, or rounds other values in their place, can miss the bound.
Values may be sent and summed in bfloat16 or wider, within the bound.
A program may use at most 64 MiB of HBM per device.

v0:
```python
import math
import jax
import jax.numpy as jnp
from jax import lax
from jax.sharding import PartitionSpec as P

NOPE = 64
ROPE = 32
VD = 64
EPS = 1e-06
THETA = 10000.0
NEG = -1e30
key_span = 2048


def norm_rows(matrix, scaling):
    mean_square = jnp.mean(matrix * matrix, axis=-1, keepdims=True)
    return matrix * lax.rsqrt(mean_square + EPS) * scaling


def rotate(matrix, places):
    half_width = matrix.shape[-1] // 2
    inverse = THETA ** (-jnp.arange(half_width, dtype=jnp.float32) / half_width)
    angles = places.astype(jnp.float32)[:, None, None] * inverse
    cosine = jnp.cos(angles)
    sine_part = jnp.sin(angles)
    leading = matrix[..., :half_width]
    trailing = matrix[..., half_width:]
    return jnp.concatenate(
        [leading * cosine - trailing * sine_part, trailing * cosine + leading * sine_part], axis=-1
    )


def doc_index(places, doc_ends):
    return jnp.sum((places[:, None] >= doc_ends[None, :]).astype(jnp.int32), axis=1)


def head_keys(latent_rows, rope_rows, places, key_up, value_up, key_gain):
    row_count = latent_rows.shape[0]
    head_count = key_up.shape[1] // NOPE
    plain_part = jnp.dot(latent_rows, key_up, preferred_element_type=jnp.float32).reshape(
        row_count, head_count, NOPE
    )
    shared_part = jnp.broadcast_to(
        rope_rows.astype(jnp.float32)[:, None, :], (row_count, head_count, ROPE)
    )
    joined = norm_rows(jnp.concatenate([plain_part, shared_part], axis=-1), key_gain)
    key_block = jnp.concatenate(
        [joined[..., :NOPE], rotate(joined[..., NOPE:], places)], axis=-1
    ).astype(jnp.bfloat16)
    value_block = jnp.dot(latent_rows, value_up, preferred_element_type=jnp.float32).astype(
        jnp.bfloat16
    )
    return (key_block, value_block.reshape(row_count, head_count, VD))


def absorb_block(running, queries, query_docs, key_block, value_block, key_docs, score_scale):
    row_top, row_total, weighted = running
    scores = (
        jnp.einsum("qhd,khd->hqk", queries, key_block, preferred_element_type=jnp.float32)
        * score_scale
    )
    allowed = (query_docs[:, None] == key_docs[None, :])[None]
    scores = jnp.where(allowed, scores, NEG)
    newest_top = jnp.maximum(row_top, jnp.max(scores, axis=-1))
    weights = jnp.where(allowed, jnp.exp(scores - newest_top[..., None]), 0.0)
    rescale = jnp.exp(row_top - newest_top)
    row_total = row_total * rescale + jnp.sum(weights, axis=-1)
    update = jnp.einsum(
        "hqk,khd->qhd",
        weights.astype(jnp.bfloat16),
        value_block,
        preferred_element_type=jnp.float32,
    )
    weighted = weighted * jnp.transpose(rescale)[:, :, None] + update
    return (newest_top, row_total, weighted)


def per_device(
    tokens,
    doc_lengths,
    query_down,
    latent_down,
    rope_down,
    query_latent_gain,
    latent_gain,
    query_up,
    key_up,
    value_up,
    query_gain,
    key_gain,
    output_gain,
    output_weight,
):
    query_latent = norm_rows(
        jnp.dot(tokens, query_down, preferred_element_type=jnp.float32), query_latent_gain
    ).astype(jnp.bfloat16)
    key_latent = norm_rows(
        jnp.dot(tokens, latent_down, preferred_element_type=jnp.float32), latent_gain
    ).astype(jnp.bfloat16)
    rope_key = jnp.dot(tokens, rope_down, preferred_element_type=jnp.float32).astype(jnp.bfloat16)
    query_rows, latent_rows, rope_rows = (
        lax.all_gather(query_latent, "tp", axis=0, tiled=True),
        lax.all_gather(key_latent, "tp", axis=0, tiled=True),
        lax.all_gather(rope_key, "tp", axis=0, tiled=True),
    )
    row_count = query_rows.shape[0]
    head_width = NOPE + ROPE
    head_count = query_up.shape[1] // head_width
    row_offset = lax.axis_index("sp") * row_count
    places = row_offset + jnp.arange(row_count, dtype=jnp.int32)
    doc_ends = jnp.cumsum(doc_lengths)
    query_docs = doc_index(places, doc_ends)
    lowest_doc = query_docs[0]
    highest_doc = query_docs[row_count - 1]
    query_raw = jnp.dot(query_rows, query_up, preferred_element_type=jnp.float32).reshape(
        row_count, head_count, head_width
    )
    query_raw = norm_rows(query_raw, query_gain)
    queries = jnp.concatenate(
        [query_raw[..., :NOPE], rotate(query_raw[..., NOPE:], places)], axis=-1
    ).astype(jnp.bfloat16)
    score_scale = head_width ** (-0.5)
    initial = (
        jnp.full((head_count, row_count), NEG, jnp.float32),
        jnp.zeros((head_count, row_count), jnp.float32),
        jnp.zeros((row_count, head_count, VD), jnp.float32),
    )

    def from_latent(sliced, key_places):
        return head_keys(sliced[0], sliced[1], key_places, key_up, value_up, key_gain)

    pieces = (
        lax.all_gather(latent_rows, "sp", axis=0, tiled=True),
        lax.all_gather(rope_rows, "sp", axis=0, tiled=True),
    )
    piece_rows = pieces[0].shape[0]
    span_rows = math.gcd(piece_rows, key_span)

    def one_span(turn_index, carried):
        offset = turn_index * span_rows
        sliced = tuple(
            (lax.dynamic_slice_in_dim(member, offset, span_rows, 0) for member in pieces)
        )
        key_places = offset + jnp.arange(span_rows, dtype=jnp.int32)
        key_docs = doc_index(key_places, doc_ends)
        touches = (key_docs[0] <= highest_doc) & (key_docs[span_rows - 1] >= lowest_doc)

        def absorb_span(current):
            key_block, value_block = from_latent(sliced, key_places)
            return absorb_block(
                current, queries, query_docs, key_block, value_block, key_docs, score_scale
            )

        def pass_over(current):
            return current

        return lax.cond(touches, absorb_span, pass_over, carried)

    row_top, row_total, weighted = lax.fori_loop(0, piece_rows // span_rows, one_span, initial)
    head_out = (
        (weighted / jnp.transpose(row_total)[:, :, None])
        .astype(jnp.bfloat16)
        .reshape(row_count, head_count * VD)
    )
    log_totals = row_top + jnp.log(row_total)
    every_head = lax.all_gather(head_out, "tp", axis=1, tiled=True)
    normed = norm_rows(every_head.astype(jnp.float32), output_gain).astype(jnp.bfloat16)
    layer_output = jnp.dot(normed, output_weight, preferred_element_type=jnp.float32).astype(
        jnp.bfloat16
    )
    return (layer_output, log_totals)


def solution(mesh):
    return jax.shard_map(
        per_device,
        mesh=mesh,
        in_specs=(
            P(("sp", "tp"), None),
            P(),
            P(),
            P(),
            P(),
            P(),
            P(),
            P(None, "tp"),
            P(None, "tp"),
            P(None, "tp"),
            P(),
            P(),
            P(),
            P(None, "tp"),
        ),
        out_specs=(P("sp", "tp"), P("tp", "sp")),
        check_vma=False,
    )
```

profile of v0, /device:TPU:0, one launch (start us, length us, event | category | flops | bytes accessed | tf_op | source)
XLA Modules:
  0.0 103.3 jit_solution(12043495153674618477)
XLA Ops:
  0.6 0.0 copy-start
  0.6 0.0 copy-start.1
  0.7 0.0 copy-start.9
  0.7 0.0 copy-start.2
  0.7 0.0 copy-start.11
  0.7 0.0 copy-start.12
  0.7 0.0 copy-start.10
  0.7 1.7 %copy-done = bf16[2048,512]{1,0:T(8,128)(2,1)S(1)} copy-done((bf16[2048,512]{1,0:T(8,128)(2,1)S(1)}, bf16[2048,512]{1,0:T(8,128)(2,1)}, u32[]{:S(2)}) %copy-start) | copy-done | bytes 2097176
  2.4 1.5 %multiply_reduce_fusion.2 = (f32[32]{0:T(128)S(1)}, f32[32,512]{1,0:T(8,128)S(1)}) fusion(bf16[32,2048]{1,0:T(8,128)(2,1)} %param.16, bf16[2048,512]{1,0:T(8,128)(2,1)S(1)} %copy-done), kind=kOutput, calls=%fused_computation.49 | convolution fusion | flops 67141600 | bytes 2293888 | tf_op jit(solution)/shard_map/dot_general | solution.py:96
  3.8 0.0 copy-start.3
  3.9 0.0 copy-start.4
  3.9 0.0 copy-done.9
  3.9 0.1 multiply_convert_fusion
  4.0 6.5 %all_gather.22 = bf16[128,512]{1,0:T(8,128)(2,1)S(1)} all-gather(bf16[32,512]{1,0:T(8,128)(2,1)S(1)} %multiply_convert_fusion), channel_id=1, replica_groups=mesh['sp'=8,'tp'=4] {'tp'}, dimensions={0}, use_global_device_ids=true | all-gather | bytes 163840 | tf_op jit(solution)/shard_map/all_gather | solution.py:103
  10.5 0.0 copy-done.2
  10.5 0.2 fusion.28
  10.7 0.0 copy-done.11
  10.7 0.1 multiply_multiply_fusion.1
  10.8 0.1 multiply_cosine_fusion.2
  11.0 0.6 pad_maximum_fusion.1
  11.6 0.0 copy-done.12
  11.6 0.1 copy.29
  11.8 0.1 reduce
  11.9 0.1 convert_reduce_fusion.1
  12.0 0.0 copy-done.1
  12.0 1.6 %multiply_reduce_fusion.3 = (f32[32]{0:T(128)S(1)}, f32[32,256]{1,0:T(8,128)S(1)}) fusion(bf16[32,2048]{1,0:T(8,128)(2,1)S(1)} %copy-done.1, bf16[2048,256]{1,0:T(8,128)(2,1)} %param.19), kind=kOutput, calls=%fused_computation.54 | convolution fusion | flops 33570784 | bytes 1212544 | tf_op jit(solution)/shard_map/dot_general | solution.py:99
  13.6 0.0 copy-done.10
  13.6 0.1 multiply_convert_fusion.1
  13.7 5.4 %all_gather.18 = bf16[128,256]{1,0:T(8,128)(2,1)S(1)} all-gather(bf16[32,256]{1,0:T(8,128)(2,1)S(1)} %multiply_convert_fusion.1), channel_id=1, replica_groups=mesh['sp'=8,'tp'=4] {'tp'}, dimensions={0}, use_global_device_ids=true | all-gather | bytes 81920 | tf_op jit(solution)/shard_map/all_gather | solution.py:104
  19.1 32.1 %all_gather.19 = bf16[1024,256]{1,0:T(8,128)(2,1)S(1)} all-gather(bf16[128,256]{1,0:T(8,128)(2,1)S(1)} %all_gather.18), channel_id=1, replica_groups=mesh['sp'=8,'tp'=4] {'sp'}, dimensions={0}, use_global_device_ids=true | all-gather | bytes 589824 | tf_op jit(solution)/shard_map/all_gather | solution.py:134
  51.2 0.1 convert_reduce_fusion
  51.3 0.0 copy-done.3
  51.3 0.2 convolution_convert_fusion.2
  51.4 5.2 %all_gather.20 = bf16[128,32]{1,0:T(8,128)(2,1)S(1)} all-gather(bf16[32,32]{1,0:T(8,128)(2,1)S(1)} %convolution_convert_fusion.2), channel_id=1, replica_groups=mesh['sp'=8,'tp'=4] {'tp'}, dimensions={0}, use_global_device_ids=true | all-gather | bytes 10240 | tf_op jit(solution)/shard_map/all_gather | solution.py:105
  56.6 30.7 %all_gather.21 = bf16[1024,32]{1,0:T(8,128)(2,1)S(1)} all-gather(bf16[128,32]{1,0:T(8,128)(2,1)S(1)} %all_gather.20), channel_id=1, replica_groups=mesh['sp'=8,'tp'=4] {'sp'}, dimensions={0}, use_global_device_ids=true | all-gather | bytes 73728 | tf_op jit(solution)/shard_map/all_gather | solution.py:135
  87.4 0.6 fusion.25
  90.5 0.0 copy-done.4
  90.5 4.6 %conditional.1 = (f32[2,128]{1,0:T(2,128)S(1)}, f32[128,2,64]{0,2,1:T(8,128)S(1)}, f32[2,128]{1,0:T(2,128)S(1)}) conditional(s32[]{:T(128)} %bitcast.1, (f32[2,128]{1,0:T(2,128)S(1)}, f32[2,128]{1,0:T(2,128)S(1)}, f32[128,2,64]{0,2,1:T(8,128)S(1)}) %tuple.27, (s32[128]{0:T(128)S(1)}, s32[1024]{0:T(1024)S(1)}, ...), branch_computations={%region_6.7_spmd.clone, %region_7.11_spmd.clone} | conditional | flops 223451936 | bytes 11297928 | solution.py:158
  90.6 0.0 copy-start.7
  90.6 0.6 copy-done.7
  91.1 0.3 fusion.27
  91.5 0.1 copy.30
  91.6 0.0 copy-start.8
  91.6 0.0 copy-start.6
  91.6 0.1 multiply_reduce_fusion
  91.7 0.8 multiply_multiply_fusion
  92.5 0.0 copy-start.5
  92.6 0.9 multiply_cosine_fusion.1
  93.6 0.0 copy-done.8
  93.6 0.2 broadcast_compare_fusion
  93.8 0.0 copy-done.6
  93.8 0.4 fusion.24
  94.2 0.0 copy-done.5
  94.2 0.3 convolution_convert_fusion
  94.5 0.4 fusion.2
  94.9 0.2 fusion.4
  95.2 0.6 log_add_fusion
  95.8 5.4 %all_gather.23 = bf16[128,512]{0,1:T(8,128)(2,1)S(1)} all-gather(bf16[128,128]{0,1:T(8,128)(2,1)S(1)} %bitcast.37), channel_id=1, replica_groups=mesh['sp'=8,'tp'=4] {'tp'}, dimensions={1}, use_global_device_ids=true | all-gather | bytes 163840 | tf_op jit(solution)/shard_map/all_gather | solution.py:167
  101.2 0.1 fusion.17
  101.3 2.1 %convolution_convert_fusion.1 = bf16[128,512]{1,0:T(8,128)(2,1)} fusion(bf16[512,512]{1,0:T(8,128)(2,1)} %param.29, bf16[128,512]{0,1:T(8,128)(2,1)S(1)} %all_gather.23, f32[512]{0:T(512)} %param.28, f32[128]{0:T(128)S(1)} %add_rsqrt_fusion.2), kind=kOutput, calls=%fused_computation.35 | convolution fusion | flops 67436544 | bytes 788992 | tf_op jit(solution)/shard_map/dot_general | solution.py:169
  (28 shorter events, 0.3 us)
Async XLA Ops:
  0.6 1.7 %copy-start = (bf16[2048,512]{1,0:T(8,128)(2,1)S(1)}, bf16[2048,512]{1,0:T(8,128)(2,1)}, u32[]{:S(2)}) copy-start(bf16[2048,512]{1,0:T(8,128)(2,1)} %param.18) | copy-start | bytes 6291460
  0.6 11.3 %copy-start.1 = (bf16[32,2048]{1,0:T(8,128)(2,1)S(1)}, bf16[32,2048]{1,0:T(8,128)(2,1)}, u32[]{:S(2)}) copy-start(bf16[32,2048]{1,0:T(8,128)(2,1)} %param.16) | copy-start | bytes 393220
  0.7 3.2 %copy-start.9 = (f32[512]{0:T(512)S(1)}, f32[512]{0:T(512)}, u32[]{:S(2)}) copy-start(f32[512]{0:T(512)} %param.21) | copy-start | bytes 6148
  0.7 9.8 %copy-start.2 = (bf16[512,192]{0,1:T(8,128)(2,1)S(1)}, bf16[512,192]{0,1:T(8,128)(2,1)}, u32[]{:S(2)}) copy-start(bf16[512,192]{0,1:T(8,128)(2,1)} %param.23) | copy-start | bytes 589828
  0.7 10.1 %copy-start.11 = (f32[96]{0:T(128)S(1)}, f32[96]{0:T(128)}, u32[]{:S(2)}) copy-start(f32[96]{0:T(128)} %param.26) | copy-start | bytes 1156
  0.7 10.9 %copy-start.12 = (s32[16]{0:T(128)S(1)}, s32[16]{0:T(128)}, u32[]{:S(2)}) copy-start(s32[16]{0:T(128)} %param.17) | copy-start | bytes 196
  0.7 12.9 %copy-start.10 = (f32[256]{0:T(256)S(1)}, f32[256]{0:T(256)}, u32[]{:S(2)}) copy-start(f32[256]{0:T(256)} %param.22) | copy-start | bytes 3076
  3.8 47.4 %copy-start.3 = (bf16[2048,32]{0,1:T(8,128)(2,1)S(1)}, bf16[2048,32]{0,1:T(8,128)(2,1)}, u32[]{:S(2)}) copy-start(bf16[2048,32]{0,1:T(8,128)(2,1)} %param.20) | copy-start | bytes 393220
  3.9 86.7 %copy-start.4 = (bf16[256,128]{1,0:T(8,128)(2,1)S(1)}, bf16[256,128]{1,0:T(8,128)(2,1)}, u32[]{:S(2)}) copy-start(bf16[256,128]{1,0:T(8,128)(2,1)} %param.24) | copy-start | bytes 196612
  90.6 0.6 copy-start.7
  91.6 2.0 %copy-start.8 = (s32[128]{0:T(128)S(1)}, s32[128]{0:T(128)}, u32[]{:S(2)}) copy-start(s32[128]{0:T(128)} %copy-done.7) | copy-start | bytes 1540 | tf_op jit(solution)/shard_map/while/body/eval_jaxpr/cond
  91.6 2.2 %copy-start.6 = (bf16[128,2,96]{0,2,1:T(8,128)(2,1)S(1)}, bf16[128,2,96]{0,2,1:T(8,128)(2,1)}, u32[]{:S(2)}) copy-start(bf16[128,2,96]{0,2,1:T(8,128)(2,1)} %get-tuple-element.141) | copy-start | bytes 147460 | tf_op jit(solution)/shard_map/while/body/eval_jaxpr/cond
  92.5 1.7 %copy-start.5 = (bf16[256,128]{1,0:T(8,128)(2,1)S(1)}, bf16[256,128]{1,0:T(8,128)(2,1)}, u32[]{:S(2)}) copy-start(bf16[256,128]{1,0:T(8,128)(2,1)} %get-tuple-element.146) | copy-start | bytes 196612 | tf_op jit(solution)/shard_map/while/body/eval_jaxpr/cond
where the time goes:
time: 104 us; the launch traced here: 103 us
  blocking collectives  85.3 us (82%)
  matrix products  6.87 us (7%)
  other arithmetic  4.36 us (4%)
  between operations  3.4 us (3%)
  local copies, waits for them, and re-layouts  3.18 us (3%)
    all_gather x1, blocking collectives, per_device(): lax.all_gather(latent_rows, 'sp', axis=0, tiled=True)  32.1 us
    all_gather x1, blocking collectives, per_device(): lax.all_gather(rope_rows, 'sp', axis=0, tiled=True)  30.7 us
    all_gather x1, blocking collectives, per_device(): lax.all_gather(query_latent, 'tp', axis=0, tiled=True)  6.49 us
    all_gather x1, blocking collectives, per_device(): every_head = lax.all_gather(head_out, 'tp', axis=1, tiled=True)  5.42 us
    all_gather x1, blocking collectives, per_device(): lax.all_gather(key_latent, 'tp', axis=0, tiled=True)  5.39 us
    all_gather x1, blocking collectives, per_device(): lax.all_gather(rope_key, 'tp', axis=0, tiled=True)  5.19 us

commit v1 on v0

--- a/solution.py
+++ b/solution.py
@@ -132,7 +132,9 @@
 
     pieces = (
         lax.all_gather(latent_rows, "sp", axis=0, tiled=True),
-        lax.all_gather(rope_rows, "sp", axis=0, tiled=True),
+        jnp.concatenate(
+            lax.all_to_all(jnp.stack([rope_rows] * lax.axis_size("sp")), "sp", 0, 0), axis=0
+        ),
     )
     piece_rows = pieces[0].shape[0]
     span_rows = math.gcd(piece_rows, key_span)

time: 104 us -> 75 us (0.72)
  blocking collectives: 85.3 us -> 54.3 us
  starting transfers between devices: 0 us -> 6.3 us
  local copies, waits for them, and re-layouts: 3.18 us -> 1.59 us
  other arithmetic: 4.36 us -> 3.14 us
  matrix products: 6.87 us -> 5.74 us
    all_gather x1 -> x0, blocking collectives: 30.7 us -> none  [per_device(): lax.all_gather(rope_rows, 'sp', axis=0, tiled=True)]
    all_to_all x0 -> x1, starting transfers between devices: none -> 6.3 us  [per_device(): lax.all_to_all(jnp.stack([rope_rows] * lax.axis_size('sp')), 'sp', 0, 0)]
    unnamed x18 -> x24, local copies, waits for them, and re-layouts: 1.71 us -> 0.07 us
    dot_general x1, matrix products: 1.62 us -> 0.39 us  [per_device(): jnp.dot(tokens, latent_down, preferred_element_type=jnp.float32)]
    dot_general x1, matrix products: 0.16 us -> 1.27 us  [per_device(): jnp.dot(tokens, rope_down, preferred_element_type=jnp.float32)]
    all_gather x1, blocking collectives: 6.49 us -> 5.4 us  [per_device(): lax.all_gather(query_latent, 'tp', axis=0, tiled=True)]
    dot_general x1, matrix products: 2.06 us -> 1 us  [per_device(): jnp.dot(normed, output_weight, preferred_element_type=jnp.float32)]
  transfers between devices with their start and end apart: 0 -> 1, of which waited for: 0 -> 0; matrix products, arithmetic and copies ran while one was open for 0% -> 5% of each run, Pallas kernels for 0% -> 0%
where the time goes in v1:
time: 75 us; the launch traced here: 74.7 us
  blocking collectives  54.3 us (72%)
  starting transfers between devices  6.3 us (8%)
  matrix products  5.74 us (8%)
  between operations  3.47 us (5%)
  other arithmetic  3.14 us (4%)
  local copies, waits for them, and re-layouts  1.59 us (2%)
    all_gather x1, blocking collectives, per_device(): lax.all_gather(latent_rows, 'sp', axis=0, tiled=True)  32 us
    all_to_all x1, starting transfers between devices, per_device(): lax.all_to_all(jnp.stack([rope_rows] * lax.axis_size('sp')), 'sp', 0, 0)  6.3 us
    all_gather x1, blocking collectives, per_device(): lax.all_gather(rope_key, 'tp', axis=0, tiled=True)  6.21 us
    all_gather x1, blocking collectives, per_device(): every_head = lax.all_gather(head_out, 'tp', axis=1, tiled=True)  5.42 us
    all_gather x1, blocking collectives, per_device(): lax.all_gather(query_latent, 'tp', axis=0, tiled=True)  5.4 us
    all_gather x1, blocking collectives, per_device(): lax.all_gather(key_latent, 'tp', axis=0, tiled=True)  5.22 us
    dot_general x1, matrix products, per_device(): jnp.dot(tokens, query_down, preferred_element_type=jnp.float32)  1.5 us
  transfers between devices with their start and end apart: 1, of which 0 were waited for; matrix products, arithmetic and copies ran while one was open for 5% of the time, Pallas kernels for 0%

profile of v1, /device:TPU:0, one launch (start us, length us, event | category | flops | bytes accessed | tf_op | source)
XLA Modules:
  0.0 74.7 jit_solution(6458029382664529090)
XLA Ops:
  0.6 0.0 copy-start
  0.6 0.0 copy-start.1
  0.7 0.0 copy-start.8
  0.7 0.0 copy-start.12
  0.7 0.0 copy-start.2
  0.7 1.3 %convolution_convert_fusion.2 = bf16[32,32]{1,0:T(8,128)(2,1)S(1)} fusion(bf16[32,2048]{1,0:T(8,128)(2,1)} %param.16, bf16[2048,32]{0,1:T(8,128)(2,1)} %param.20), kind=kOutput, calls=%fused_computation.38 | convolution fusion | flops 4195328 | bytes 264192 | tf_op jit(solution)/shard_map/dot_general | solution.py:101
  2.0 6.2 %all_gather.17 = bf16[128,32]{1,0:T(8,128)(2,1)S(1)} all-gather(bf16[32,32]{1,0:T(8,128)(2,1)S(1)} %convolution_convert_fusion.2), channel_id=1, replica_groups=mesh['sp'=8,'tp'=4] {'tp'}, dimensions={0}, use_global_device_ids=true | all-gather | bytes 10240 | tf_op jit(solution)/shard_map/all_gather | solution.py:105
  8.2 0.1 copy.34
  8.2 0.7 stack.2
  8.9 6.3 %all-to-all-start = ((bf16[8,128,32]{1,2,0:T(8,128)(2,1)}), bf16[8,128,32]{1,2,0:T(8,128)(2,1)S(1)}, u32[]{:S(2)}, u32[]{:S(2)}) async-start(bf16[8,128,32]{1,2,0:T(8,128)(2,1)} %stack.2), calls=%async_computation | async-start | bytes 131072 | tf_op jit(solution)/shard_map/all_to_all | solution.py:136
  15.2 0.0 copy-start.4
  15.2 0.0 copy-done
  15.3 0.0 copy-start.9
  15.3 0.0 copy-start.10
  15.3 1.5 %multiply_reduce_fusion.2 = (f32[32]{0:T(128)S(1)}, f32[32,512]{1,0:T(8,128)S(1)}) fusion(bf16[32,2048]{1,0:T(8,128)(2,1)} %param.16, bf16[2048,512]{1,0:T(8,128)(2,1)S(1)} %copy-done), kind=kOutput, calls=%fused_computation.51 | convolution fusion | flops 67141600 | bytes 2293888 | tf_op jit(solution)/shard_map/dot_general | solution.py:96
  16.8 0.0 copy-start.5
  16.8 0.0 copy-start.11
  16.8 0.0 copy-done.8
  16.8 0.1 multiply_convert_fusion
  16.9 5.4 %all_gather.18 = bf16[128,512]{1,0:T(8,128)(2,1)S(1)} all-gather(bf16[32,512]{1,0:T(8,128)(2,1)S(1)} %multiply_convert_fusion), channel_id=1, replica_groups=mesh['sp'=8,'tp'=4] {'tp'}, dimensions={0}, use_global_device_ids=true | all-gather | bytes 163840 | tf_op jit(solution)/shard_map/all_gather | solution.py:103
  22.3 0.0 copy-done.4
  22.3 0.2 fusion.28
  22.6 0.0 copy-done.12
  22.6 0.1 copy.33
  22.7 0.1 reduce
  22.8 0.1 convert_reduce_fusion
  22.9 0.1 convert_reduce_fusion.1
  23.0 0.0 copy-done.1
  23.0 0.0 copy-done.2
  23.0 0.4 multiply_reduce_fusion.3
  23.4 0.0 copy-done.9
  23.4 0.1 multiply_convert_fusion.1
  23.5 5.2 %all_gather.15 = bf16[128,256]{1,0:T(8,128)(2,1)S(1)} all-gather(bf16[32,256]{1,0:T(8,128)(2,1)S(1)} %multiply_convert_fusion.1), channel_id=1, replica_groups=mesh['sp'=8,'tp'=4] {'tp'}, dimensions={0}, use_global_device_ids=true | all-gather | bytes 81920 | tf_op jit(solution)/shard_map/all_gather | solution.py:104
  28.7 32.0 %all_gather.16 = bf16[1024,256]{1,0:T(8,128)(2,1)S(1)} all-gather(bf16[128,256]{1,0:T(8,128)(2,1)S(1)} %all_gather.15), channel_id=1, replica_groups=mesh['sp'=8,'tp'=4] {'sp'}, dimensions={0}, use_global_device_ids=true | all-gather | bytes 589824 | tf_op jit(solution)/shard_map/all_gather | solution.py:134
  60.8 0.0 copy-done.10
  60.8 0.1 multiply_multiply_fusion.1
  60.9 0.1 multiply_cosine_fusion.2
  61.0 0.6 fusion.25
  64.2 0.0 all-to-all-done
  64.2 0.0 copy-done.5
  64.2 0.0 copy-done.11
  64.2 0.0 copy-start.3
  64.2 0.0 copy-start.7
  64.2 3.3 %conditional.1 = (f32[2,128]{1,0:T(2,128)S(1)}, f32[128,2,64]{0,2,1:T(8,128)S(1)}, f32[2,128]{1,0:T(2,128)S(1)}) conditional(s32[]{:T(128)} %bitcast.1, (f32[2,128]{1,0:T(2,128)S(1)}, f32[2,128]{1,0:T(2,128)S(1)}, f32[128,2,64]{0,2,1:T(8,128)S(1)}) %tuple.27, (s32[128]{0:T(128)S(1)}, s32[1024]{0:T(1024)S(1)}, ...), branch_computations={%region_6.7_spmd.clone, %region_7.11_spmd.clone} | conditional | flops 223484704 | bytes 11490356 | solution.py:160
  64.3 0.3 fusion.27
  64.7 0.1 multiply_reduce_fusion
  64.8 0.1 multiply_multiply_fusion
  64.9 0.0 copy-start.6
  65.0 0.9 %multiply_cosine_fusion.1 = (f32[1024,16]{0,1:T(8,128)S(1)}, f32[1024,16]{0,1:T(8,128)S(1)}, f32[1024,16]{0,1:T(8,128)S(1)}, f32[1024,16]{0,1:T(8,128)S(1)}) fusion(f32[16]{0:T(128)S(1)} %multiply_power_fusion, f32[1024]{0:T(1024)S(1)} %convert_element_type.79, f32[1024]{0:T(1024)S(1)} %convert_element_type.80, f32[1024]{0:T(1024)S(1)} %convert_element_type.81, ...), kind=kLoop, calls=%fused_computation.29 | loop fusion | flops 65536 | bytes 278592 | tf_op jit(solution)/shard_map/while/body/eval_jaxpr/cond/branch_1_fun/cos | solution.py:25
  66.0 0.2 broadcast_compare_fusion
  66.2 0.4 fusion.24
  66.6 0.0 copy-done.6
  66.6 0.3 convolution_convert_fusion
  66.9 0.4 fusion.2
  67.3 0.2 fusion.4
  67.6 0.6 log_add_fusion
  68.2 5.4 %all_gather.19 = bf16[128,512]{0,1:T(8,128)(2,1)S(1)} all-gather(bf16[128,128]{0,1:T(8,128)(2,1)S(1)} %bitcast.45), channel_id=1, replica_groups=mesh['sp'=8,'tp'=4] {'tp'}, dimensions={1}, use_global_device_ids=true | all-gather | bytes 163840 | tf_op jit(solution)/shard_map/all_gather | solution.py:169
  73.6 0.1 fusion.17
  73.7 0.0 copy-done.3
  73.7 0.0 copy-done.7
  73.7 1.0 %convolution_convert_fusion.1 = bf16[128,512]{1,0:T(8,128)(2,1)} fusion(bf16[512,512]{1,0:T(8,128)(2,1)S(1)} %copy-done.3, bf16[128,512]{0,1:T(8,128)(2,1)S(1)} %all_gather.19, f32[512]{0:T(512)S(1)} %copy-done.7, f32[128]{0:T(128)S(1)} %add_rsqrt_fusion.2), kind=kOutput, calls=%fused_computation.37 | convolution fusion | flops 67436544 | bytes 788992 | tf_op jit(solution)/shard_map/dot_general | solution.py:171
  (31 shorter events, 0.4 us)
Async XLA Ops:
  0.6 14.6 %copy-start = (bf16[2048,512]{1,0:T(8,128)(2,1)S(1)}, bf16[2048,512]{1,0:T(8,128)(2,1)}, u32[]{:S(2)}) copy-start(bf16[2048,512]{1,0:T(8,128)(2,1)} %param.18) | copy-start | bytes 6291460
  0.6 22.4 %copy-start.1 = (bf16[32,2048]{1,0:T(8,128)(2,1)S(1)}, bf16[32,2048]{1,0:T(8,128)(2,1)}, u32[]{:S(2)}) copy-start(bf16[32,2048]{1,0:T(8,128)(2,1)} %param.16) | copy-start | bytes 393220
  0.7 16.2 %copy-start.8 = (f32[512]{0:T(512)S(1)}, f32[512]{0:T(512)}, u32[]{:S(2)}) copy-start(f32[512]{0:T(512)} %param.21) | copy-start | bytes 6148
  0.7 21.9 %copy-start.12 = (s32[16]{0:T(128)S(1)}, s32[16]{0:T(128)}, u32[]{:S(2)}) copy-start(s32[16]{0:T(128)} %param.17) | copy-start | bytes 196
  0.7 22.3 %copy-start.2 = (bf16[2048,256]{1,0:T(8,128)(2,1)S(1)}, bf16[2048,256]{1,0:T(8,128)(2,1)}, u32[]{:S(2)}) copy-start(bf16[2048,256]{1,0:T(8,128)(2,1)} %param.19) | copy-start | bytes 3145732
  8.9 55.3 %all-to-all-start = ((bf16[8,128,32]{1,2,0:T(8,128)(2,1)}), bf16[8,128,32]{1,2,0:T(8,128)(2,1)S(1)}, u32[]{:S(2)}, u32[]{:S(2)}) async-start(bf16[8,128,32]{1,2,0:T(8,128)(2,1)} %stack.2), calls=%async_computation | async-start | bytes 131072 | tf_op jit(solution)/shard_map/all_to_all | solution.py:136
  15.2 7.1 %copy-start.4 = (bf16[512,192]{0,1:T(8,128)(2,1)S(1)}, bf16[512,192]{0,1:T(8,128)(2,1)}, u32[]{:S(2)}) copy-start(bf16[512,192]{0,1:T(8,128)(2,1)} %param.23) | copy-start | bytes 589828
  15.3 8.2 %copy-start.9 = (f32[256]{0:T(256)S(1)}, f32[256]{0:T(256)}, u32[]{:S(2)}) copy-start(f32[256]{0:T(256)} %param.22) | copy-start | bytes 3076
  15.3 45.5 %copy-start.10 = (f32[96]{0:T(128)S(1)}, f32[96]{0:T(128)}, u32[]{:S(2)}) copy-start(f32[96]{0:T(128)} %param.26) | copy-start | bytes 1156
  16.8 47.4 %copy-start.5 = (bf16[256,128]{1,0:T(8,128)(2,1)S(1)}, bf16[256,128]{1,0:T(8,128)(2,1)}, u32[]{:S(2)}) copy-start(bf16[256,128]{1,0:T(8,128)(2,1)} %param.24) | copy-start | bytes 196612
  16.8 47.4 %copy-start.11 = (f32[96]{0:T(128)S(1)}, f32[96]{0:T(128)}, u32[]{:S(2)}) copy-start(f32[96]{0:T(128)} %param.27) | copy-start | bytes 1156
  64.2 9.4 %copy-start.3 = (bf16[512,512]{1,0:T(8,128)(2,1)S(1)}, bf16[512,512]{1,0:T(8,128)(2,1)}, u32[]{:S(2)}) copy-start(bf16[512,512]{1,0:T(8,128)(2,1)} %param.29) | copy-start | bytes 1572868
  64.2 9.4 %copy-start.7 = (f32[512]{0:T(512)S(1)}, f32[512]{0:T(512)}, u32[]{:S(2)}) copy-start(f32[512]{0:T(512)} %param.28) | copy-start | bytes 6148
  64.9 1.7 %copy-start.6 = (bf16[256,128]{1,0:T(8,128)(2,1)S(1)}, bf16[256,128]{1,0:T(8,128)(2,1)}, u32[]{:S(2)}) copy-start(bf16[256,128]{1,0:T(8,128)(2,1)} %get-tuple-element.147) | copy-start | bytes 196612 | tf_op jit(solution)/shard_map/while/body/eval_jaxpr/cond
